TPU v7x, 512 devices: a whole 4x4x16 slice. The times are simulated.
512 devices in a mesh: ep: 128 (over z, x, core), tp: 4 (over y).
Axes of the slice: x: 4, y: 4, z: 16, core: 2. Of those that a mesh axis runs over, the one named last changes fastest.
Arguments:
- hidden_in: bfloat16 [2048, 1024], P('ep', 'tp'), may hold values from -40 to 40
- norm_gain_attn: float32 [1024], replicated, may hold values from 0.1 to 1.9
- query_weight: bfloat16 [1024, 512], P(None, 'tp'), may hold values from -0.1875 to 0.1875
- key_weight: bfloat16 [1024, 512], P(None, 'tp'), may hold values from -0.1875 to 0.1875
- value_weight: bfloat16 [1024, 512], P(None, 'tp'), may hold values from -0.1875 to 0.1875
- query_gain: float32 [128], replicated, may hold values from 1 to 1.6
- key_gain: float32 [128], replicated, may hold values from 1 to 1.6
- lambda_head: float32 [4], P('tp'), may hold values from 0.3 to 0.8
- sub_gain: float32 [128], replicated, may hold values from 0.1 to 1.9
- out_weight: bfloat16 [512, 1024], P('tp'), may hold values from -0.25 to 0.25
- cache_key: bfloat16 [2048, 256, 512], P('ep', None, 'tp'), may hold values from -8 to 8
- cache_value: bfloat16 [2048, 256, 512], P('ep', None, 'tp'), may hold values from -6 to 6
- lengths: int32 [2048], P('ep'), may hold values from 1 to 256
- norm_gain_mix: float32 [1024], P('tp'), may hold values from 0.1 to 1.9
- route_ids: int32 [2048, 6], P('ep'), may hold values from 0 to 127, all different within a row; in each aligned block of 16 rows (0 to 15, 16 to 31, ...) at most 2 rows name the same one
- route_logits: float32 [2048, 6], P('ep'), may hold values from -4 to 4
- expert_gate: bfloat16 [128, 1024, 1024], P('ep', None, 'tp'), may hold values from -0.5 to 0.5
- expert_up: bfloat16 [128, 1024, 1024], P('ep', None, 'tp'), may hold values from -0.5 to 0.5
- expert_down: bfloat16 [128, 1024, 1024], P('ep', 'tp'), may hold values from -0.046875 to 0.046875
- dense_gate: bfloat16 [1024, 2048], P('tp', 'ep'), may hold values from -0.1875 to 0.1875
- dense_up: bfloat16 [1024, 2048], P('tp', 'ep'), may hold values from -0.1875 to 0.1875
- dense_down: bfloat16 [2048, 1024], P('ep', 'tp'), may hold values from -0.125 to 0.125
- branch_gate: float32 [1024], P('tp'), may hold values from -0.1875 to 0.1875
Outputs:
- layer_out: bfloat16 [2048, 1024], P('ep', 'tp')
- key_rows: bfloat16 [2048, 512], P('ep', 'tp')
- value_rows: bfloat16 [2048, 512], P('ep', 'tp')
Inputs may be any that keep to these rules, and one draw needn't show every extreme that they name: `route_ids`: each row names 6 different experts. Among the rows of one index of ep (aligned blocks of 16 rows) no expert is named by more than 2 rows, and in some blocks one expert is named by exactly 2.
All inputs are finite; a program needn't handle non-finite values.
Results may differ from a plain program's by a relative error of at most 0.0075.
Values may be sent and summed in bfloat16 or wider, within the bound.
No kernel may reach another device: no remote copies, remote signals or barrier semaphores. Data moves between devices by JAX's collectives and lax.ppermute only.
A program may use at most 64 MiB of HBM per device.

v0:
```python
import math
import jax
import jax.numpy as jnp
from jax import lax
from jax.sharding import Mesh
from jax.sharding import PartitionSpec as P

EP = ("ep_0", "ep_1", "ep_2")
EPSILON = 1e-06
CLAMP_LIMIT = 7.0
SWISH_ALPHA = 1.702
OUT_SCALE = 0.2 + 0.6 * math.exp(-0.6)


def laid_out(blocks, dim):
    blocks = jnp.moveaxis(blocks, 0, dim)
    dims = blocks.shape
    return blocks.reshape(*dims[:dim], dims[dim] * dims[dim + 1], *dims[dim + 2 :])


def from_everyone(x, axis):
    copies = jnp.broadcast_to(x, (lax.axis_size(axis), *x.shape))
    return lax.all_to_all(copies, axis, split_axis=0, concat_axis=0, tiled=True)


def collect(x, axis, dim):
    return laid_out(from_everyone(x, axis), dim)


def cut_along(x, dim, length):
    dims = x.shape
    blocks = x.reshape(*dims[:dim], length, dims[dim] // length, *dims[dim + 1 :])
    return jnp.moveaxis(blocks, dim, 0)


def summed_on_arrival(x, axis, dim):
    length = lax.axis_size(axis)
    blocks = lax.all_to_all(cut_along(x, dim, length), axis, 0, 0, tiled=True)
    return jnp.sum(blocks, axis=0)


def taken_together(x, axis):
    return from_everyone(x, axis).sum(axis=0)


def together(arrays, axis):
    ends = [0]
    for a in arrays:
        ends.append(ends[-1] + a.size)
    subtotal = taken_together(jnp.concatenate([a.ravel() for a in arrays]), axis)
    return tuple((subtotal[b:e].reshape(a.shape) for a, b, e in zip(arrays, ends, ends[1:])))


def gather_turned(arrays, axis, dims):
    turned = [jnp.moveaxis(a, dim, 0) for a, dim in zip(arrays, dims)]
    both = jnp.concatenate([t.reshape(len(t), -1) for t in turned], axis=1)
    whole, at, done = (lax.all_gather(both, axis, axis=0, tiled=True), 0, [])
    for t, dim in zip(turned, dims):
        section = whole[:, at : at + t[0].size].reshape(-1, *t.shape[1:])
        done.append(jnp.moveaxis(section, 0, dim))
        at += t[0].size
    return tuple(done)


def stacked_from(x, axes, sequence):
    blocks = x[None]
    for k in sequence:
        blocks = lax.all_gather(blocks, axes[k], axis=0, tiled=True)
    block = [lax.axis_size(axes[k]) for k in reversed(sequence)]
    blocks = blocks.reshape(*block, *x.shape)
    turned = sorted(range(len(sequence)), key=lambda place: sequence[len(sequence) - 1 - place])
    return blocks.transpose(*turned, *range(len(sequence), blocks.ndim)).reshape(-1, *x.shape)


def whole_of(x, axes, sequence, dim):
    return laid_out(stacked_from(x, axes, sequence), dim)


def rms_scale(values, scale_gain):
    mean_square = jnp.mean(values * values, axis=-1, keepdims=True)
    return values * lax.rsqrt(mean_square + EPSILON) * scale_gain


def clamped_unit(gate_pre, up_pre):
    gate_cut = jnp.minimum(gate_pre, CLAMP_LIMIT)
    up_cut = jnp.clip(up_pre, -CLAMP_LIMIT, CLAMP_LIMIT)
    return (up_cut + 1.0) * gate_cut * jax.nn.sigmoid(SWISH_ALPHA * gate_cut)


def attend(
    normed,
    query_weight,
    key_weight,
    value_weight,
    query_gain,
    key_gain,
    lambda_head,
    sub_gain,
    cache_key,
    cache_value,
    lengths,
):
    seq_count = normed.shape[0]
    head_count = lambda_head.shape[0]
    qk_size = query_gain.shape[0] // 2
    val_size = value_weight.shape[1] // head_count
    cache_len = cache_key.shape[1]
    scale_factor = qk_size ** (-0.5)
    query_pre = jnp.dot(normed, query_weight, preferred_element_type=jnp.float32)
    query_rows = rms_scale(
        query_pre.reshape(seq_count, head_count, 2, qk_size), query_gain.reshape(2, qk_size)
    ).astype(jnp.bfloat16)
    key_pre = jnp.dot(normed, key_weight, preferred_element_type=jnp.float32)
    key_rows = rms_scale(
        key_pre.reshape(seq_count, head_count, 2, qk_size), key_gain.reshape(2, qk_size)
    ).astype(jnp.bfloat16)
    value_rows = jnp.dot(normed, value_weight, preferred_element_type=jnp.float32).astype(
        jnp.bfloat16
    )
    key_past = cache_key.reshape(seq_count, cache_len, head_count, 2, qk_size)
    past_score = (
        jnp.einsum("shmd,sjhmd->shmj", query_rows, key_past, preferred_element_type=jnp.float32)
        * scale_factor
    )
    own_score = (
        jnp.einsum("shmd,shmd->shm", query_rows, key_rows, preferred_element_type=jnp.float32)
        * scale_factor
    )
    valid_mask = lax.iota(jnp.int32, cache_len)[None, :] < lengths[:, None]
    past_exp = jnp.where(valid_mask[:, None, None, :], jnp.exp(past_score), 0.0)
    own_exp = jnp.exp(own_score)
    denominator = jnp.sum(past_exp, axis=-1) + own_exp
    past_prob = past_exp / denominator[..., None]
    own_prob = own_exp / denominator
    weight_past = (past_prob[:, :, 0] - lambda_head[None, :, None] * past_prob[:, :, 1]).astype(
        jnp.bfloat16
    )
    weight_own = (own_prob[:, :, 0] - lambda_head[None, :] * own_prob[:, :, 1]).astype(jnp.bfloat16)
    value_past = cache_value.reshape(seq_count, cache_len, head_count, val_size)
    head_mix = jnp.einsum(
        "shj,sjhe->she", weight_past, value_past, preferred_element_type=jnp.float32
    )
    own_value = value_rows.reshape(seq_count, head_count, val_size).astype(jnp.float32)
    head_mix = head_mix + weight_own.astype(jnp.float32)[..., None] * own_value
    head_out = (rms_scale(head_mix, sub_gain) * OUT_SCALE).astype(jnp.bfloat16)
    return (
        head_out.reshape(seq_count, head_count * val_size),
        key_rows.reshape(seq_count, -1),
        value_rows,
    )


def body(
    hidden_in,
    norm_gain_attn,
    query_weight,
    key_weight,
    value_weight,
    query_gain,
    key_gain,
    lambda_head,
    sub_gain,
    out_weight,
    cache_key,
    cache_value,
    lengths,
    norm_gain_mix,
    route_ids,
    route_logits,
    expert_gate,
    expert_up,
    expert_down,
    dense_gate,
    dense_up,
    dense_down,
    branch_gate,
):
    seq_count, top_count = route_ids.shape
    full_rows = collect(hidden_in, "tp", 1)
    width_total = full_rows.shape[1]
    normed = rms_scale(full_rows.astype(jnp.float32), norm_gain_attn).astype(jnp.bfloat16)
    head_out, key_rows, value_rows = attend(
        normed,
        query_weight,
        key_weight,
        value_weight,
        query_gain,
        key_gain,
        lambda_head,
        sub_gain,
        cache_key,
        cache_value,
        lengths,
    )
    head_terms = jnp.dot(head_out, out_weight, preferred_element_type=jnp.float32)
    attn_part = summed_on_arrival(head_terms, "tp", 1)
    residual = hidden_in.astype(jnp.float32) + attn_part
    square_sum, gate_raw = together(
        (
            jnp.sum(residual * residual, axis=1),
            jnp.sum(residual * (norm_gain_mix * branch_gate)[None, :], axis=1),
        ),
        "tp",
    )
    inverse = lax.rsqrt(square_sum / width_total + EPSILON)
    mix_float = residual * inverse[:, None] * norm_gain_mix[None, :]
    gate_logit = gate_raw * inverse
    branch_weight = jax.nn.sigmoid(gate_logit)[:, None]
    mix_rows = mix_float.astype(jnp.bfloat16)
    route_weight = jax.nn.softmax(route_logits, axis=1)
    experts = lax.axis_size(EP) * expert_gate.shape[0]
    capacity = min(seq_count, 2 * ((seq_count * top_count + experts - 1) // experts))
    flat_ids = route_ids.reshape(-1)
    one_hot = (flat_ids[:, None] == lax.iota(jnp.int32, experts)[None, :]).astype(jnp.int32)
    route_rank = jnp.sum((jnp.cumsum(one_hot, axis=0) - one_hot) * one_hot, axis=1)
    slot_index = flat_ids * capacity + route_rank
    select_matrix = (
        lax.iota(jnp.int32, experts * capacity)[:, None] == slot_index[None, :]
    ).astype(jnp.bfloat16)
    route_rows = jnp.repeat(mix_rows, top_count, axis=0)
    placed = jnp.dot(select_matrix, route_rows, preferred_element_type=jnp.float32)
    arrived = collect(
        lax.all_to_all(
            placed.astype(jnp.bfloat16).reshape(experts, capacity, mix_rows.shape[1]),
            EP,
            split_axis=0,
            concat_axis=0,
            tiled=True,
        ),
        "tp",
        2,
    )
    source_count, item_count, width_now = arrived.shape
    flat_rows = arrived.reshape(source_count * item_count, width_now)
    gate_pre = jnp.dot(flat_rows, expert_gate[0], preferred_element_type=jnp.float32)
    up_pre = jnp.dot(flat_rows, expert_up[0], preferred_element_type=jnp.float32)
    activation = clamped_unit(gate_pre, up_pre).astype(jnp.bfloat16)
    partial_out = jnp.dot(activation, expert_down[0], preferred_element_type=jnp.float32)
    partial_out = partial_out.reshape(source_count, item_count, width_now)
    summed = summed_on_arrival(partial_out, "tp", 2).astype(jnp.bfloat16)
    returned = lax.all_to_all(summed, EP, split_axis=0, concat_axis=0, tiled=True)
    local_width = returned.shape[2]
    route_out = jnp.dot(
        select_matrix.T,
        returned.reshape(experts * capacity, local_width),
        preferred_element_type=jnp.float32,
    )
    routed = jnp.sum(
        route_out.reshape(seq_count, top_count, local_width) * route_weight[:, :, None], axis=1
    )
    pieces = gather_turned((dense_gate, dense_up), EP, (1, 1))
    gate_block = jnp.dot(mix_rows, pieces[0], preferred_element_type=jnp.float32)
    up_block = jnp.dot(mix_rows, pieces[1], preferred_element_type=jnp.float32)
    gate_full, up_full = together((gate_block, up_block), "tp")
    own_act = (jax.nn.silu(gate_full) * up_full).astype(jnp.bfloat16)
    dense_result = jnp.dot(
        own_act, whole_of(dense_down, EP, (1, 0, 2), 0), preferred_element_type=jnp.float32
    )
    layer_out = (residual + routed + branch_weight * dense_result).astype(jnp.bfloat16)
    return (layer_out, key_rows, value_rows)


def solution(mesh):
    split = Mesh(mesh.devices.reshape(16, 4, 2, mesh.shape["tp"]), ("ep_0", "ep_1", "ep_2", "tp"))
    in_specs = (
        P(EP, "tp"),
        P(),
        P(None, "tp"),
        P(None, "tp"),
        P(None, "tp"),
        P(),
        P(),
        P("tp"),
        P(),
        P("tp", None),
        P(EP, None, "tp"),
        P(EP, None, "tp"),
        P(EP),
        P("tp"),
        P(EP, None),
        P(EP, None),
        P(EP, None, "tp"),
        P(EP, None, "tp"),
        P(EP, "tp", None),
        P("tp", EP),
        P("tp", EP),
        P(EP, "tp"),
        P("tp"),
    )
    out_specs = (P(EP, "tp"), P(EP, "tp"), P(EP, "tp"))
    return jax.shard_map(body, mesh=split, in_specs=in_specs, out_specs=out_specs, check_vma=False)
```

profile of v0, /device:TPU:32, one launch (start us, length us, event | category | flops | bytes accessed | tf_op | source)
XLA Modules:
  0.0 202.3 jit_solution(13070366693453311810)
XLA Ops:
  7.2 1.4 broadcast_in_dim.25
  8.6 4.5 %all-to-all-start = ((bf16[4,16,256]{2,1,0:T(8,128)(2,1)}), bf16[4,16,256]{2,1,0:T(8,128)(2,1)S(1)}, u32[]{:S(2)}, u32[]{:S(2)}) async-start(bf16[4,16,256]{2,1,0:T(8,128)(2,1)} %broadcast_in_dim.25), calls=%async_computation | async-start | bytes 65536 | tf_op jit(solution)/shard_map/all_to_all | solution.py:23
  13.1 1.3 pad_maximum_fusion.1
  14.5 0.8 copy.83
  15.4 0.7 iota_compare_fusion.4
  16.1 0.7 mul.280
  16.9 0.7 mul.289
  17.6 1.5 copy.81
  19.7 0.2 copy.104
  21.2 0.2 fusion.22
  21.5 0.2 fusion.25
  22.0 0.2 fusion.23
  22.2 1.2 multiply_reduce_fusion.2
  23.5 0.8 convolution_bitcast_fusion.3
  24.3 4.8 %all-to-all-start.1 = ((f32[4,16,256]{2,1,0:T(8,128)}), f32[4,16,256]{2,1,0:T(8,128)S(1)}, u32[]{:S(2)}, u32[]{:S(2)}) async-start(f32[4,16,256]{2,1,0:T(8,128)} %convolution_bitcast_fusion.3), calls=%async_computation.1 | async-start | bytes 131072 | tf_op jit(solution)/shard_map/all_to_all | solution.py:38
  29.1 0.2 select_reduce_fusion
  29.3 5.4 %all-to-all-done.1 = f32[4,16,256]{2,1,0:T(8,128)S(1)} async-done(((f32[4,16,256]{2,1,0:T(8,128)}), f32[4,16,256]{2,1,0:T(8,128)S(1)}, u32[]{:S(2)}, u32[]{:S(2)}) %all-to-all-start.1) | async-done | bytes 65568 | tf_op jit(solution)/shard_map/all_to_all | solution.py:38
  34.9 0.6 broadcast_in_dim.27
  35.5 3.2 %all-to-all-start.2 = ((f32[4,1,32]{2,1,0:T(1,128)}), f32[4,1,32]{2,1,0:T(1,128)S(1)}, u32[]{:S(2)}, u32[]{:S(2)}) async-start(f32[4,1,32]{2,1,0:T(1,128)} %broadcast_in_dim.27), calls=%async_computation.2 | async-start | bytes 4096 | tf_op jit(solution)/shard_map/all_to_all | solution.py:23
  38.8 5.2 %all-to-all-done.2 = f32[4,1,32]{2,1,0:T(1,128)S(1)} async-done(((f32[4,1,32]{2,1,0:T(1,128)}), f32[4,1,32]{2,1,0:T(1,128)S(1)}, u32[]{:S(2)}, u32[]{:S(2)}) %all-to-all-start.2) | async-done | bytes 544 | tf_op jit(solution)/shard_map/all_to_all | solution.py:23
  44.2 0.2 convolution_convert_fusion
  44.4 36.1 %all_to_all.42 = bf16[128,2,256]{2,1,0:T(2,128)(2,1)S(1)} all-to-all(bf16[128,2,256]{2,1,0:T(2,128)(2,1)S(1)} %reshape.305), channel_id=1, replica_groups=mesh['ep_0'=16,'ep_1'=4,'ep_2'=2,'tp'=4] {'ep_0','ep_1','ep_2'}, dimensions={0} | all-to-all | bytes 262144 | tf_op jit(solution)/shard_map/all_to_all | solution.py:223
  80.5 1.1 broadcast_in_dim.29
  81.6 3.6 %all-to-all-start.4 = ((bf16[4,128,2,256]{3,2,1,0:T(2,128)(2,1)}), bf16[4,128,2,256]{3,2,1,0:T(2,128)(2,1)S(1)}, u32[]{:S(2)}, u32[]{:S(2)}) async-start(bf16[4,128,2,256]{3,2,1,0:T(2,128)(2,1)} %broadcast_in_dim.29), calls=%async_computation.4 | async-start | bytes 1048576 | tf_op jit(solution)/shard_map/all_to_all | solution.py:23
  85.2 0.2 copy.107
  85.4 9.8 %all-to-all-done.4 = bf16[4,128,2,256]{3,2,1,0:T(2,128)(2,1)S(1)} async-done(((bf16[4,128,2,256]{3,2,1,0:T(2,128)(2,1)}), bf16[4,128,2,256]{3,2,1,0:T(2,128)(2,1)S(1)}, u32[]{:S(2)}, u32[]{:S(2)}) %all-to-all-start.4) | async-done | bytes 524320 | tf_op jit(solution)/shard_map/all_to_all | solution.py:23
  95.2 0.7 copy.85
  96.0 0.3 convolution_minimum_fusion
  96.3 0.3 fusion.3
  96.7 0.3 convolution_bitcast_fusion
  97.1 1.1 copy.88
  98.1 3.5 %all-to-all-start.5 = ((f32[4,128,2,256]{3,1,2,0:T(8,128)}), f32[4,128,2,256]{3,1,2,0:T(8,128)S(1)}, u32[]{:S(2)}, u32[]{:S(2)}) async-start(f32[4,128,2,256]{3,1,2,0:T(8,128)} %copy.88), calls=%async_computation.5 | async-start | bytes 2097152 | tf_op jit(solution)/shard_map/all_to_all | solution.py:38
  101.7 11.9 %all-gather = bf16[64,256]{1,0:T(8,128)(2,1)S(1)} all-gather(bf16[16,256]{1,0:T(8,128)(2,1)S(1)} %copy-done.8), channel_id=2, replica_groups=mesh['ep_0'=16,'ep_1'=4,'ep_2'=2,'tp'=4] {'ep_1'}, dimensions={0}, use_global_device_ids=true | all-gather | bytes 40960 | tf_op jit(solution)/shard_map/all_gather | solution.py:68
  113.6 31.7 %all_gather.14 = bf16[64,16,256]{2,1,0:T(8,128)(2,1)} all-gather(bf16[4,16,256]{2,1,0:T(8,128)(2,1)S(1)} %bitcast.104), channel_id=1, replica_groups=mesh['ep_0'=16,'ep_1'=4,'ep_2'=2,'tp'=4] {'ep_0'}, dimensions={0}, use_global_device_ids=true | all-gather | bytes 557056 | tf_op jit(solution)/shard_map/all_gather | solution.py:68
  145.4 0.8 copy.90
  146.2 8.6 %all-to-all-start.6 = ((bf16[128,2,256]{2,1,0:T(2,128)(2,1)}), bf16[128,2,256]{2,1,0:T(2,128)(2,1)S(1)}, u32[]{:S(2)}, u32[]{:S(2)}) async-start(bf16[128,2,256]{2,1,0:T(2,128)(2,1)} %copy.90), calls=%async_computation.6 | async-start | bytes 262144 | tf_op jit(solution)/shard_map/all_to_all | solution.py:241
  154.9 6.9 %all-gather.4.cloned.1.call-done = bf16[2048,512]{1,0:T(8,128)(2,1)} async-done(((bf16[16,512]{1,0:T(8,128)(2,1)}), bf16[2048,512]{1,0:T(8,128)(2,1)}) %all-gather.4.cloned.1.call-update) | async-done | bytes 2097168 | tf_op jit(solution)/shard_map/all_gather | solution.py:57
  161.8 1.6 convolution_bitcast_fusion.2
  163.4 1.6 convolution_bitcast_fusion.1
  165.1 6.8 %all-to-all-done.6 = bf16[128,2,256]{2,1,0:T(2,128)(2,1)S(1)} async-done(((bf16[128,2,256]{2,1,0:T(2,128)(2,1)}), bf16[128,2,256]{2,1,0:T(2,128)(2,1)S(1)}, u32[]{:S(2)}, u32[]{:S(2)}) %all-to-all-start.6) | async-done | bytes 131104 | tf_op jit(solution)/shard_map/all_to_all | solution.py:241
  171.9 1.5 broadcast_in_dim.30
  173.5 4.7 %all-to-all-start.7 = ((f32[4,1,65536]{2,1,0:T(1,128)}), f32[4,1,65536]{2,1,0:T(1,128)S(1)}, u32[]{:S(2)}, u32[]{:S(2)}) async-start(f32[4,1,65536]{2,1,0:T(1,128)} %broadcast_in_dim.30), calls=%async_computation.7 | async-start | bytes 2097152 | tf_op jit(solution)/shard_map/all_to_all | solution.py:23
  178.5 0.6 multiply_convert_fusion.6
  179.1 1.2 all-gather.6.cloned.1.call-done
  180.4 1.3 copy.93
  181.9 11.6 %all-to-all-done.7 = f32[4,1,65536]{2,1,0:T(1,128)S(1)} async-done(((f32[4,1,65536]{2,1,0:T(1,128)}), f32[4,1,65536]{2,1,0:T(1,128)S(1)}, u32[]{:S(2)}, u32[]{:S(2)}) %all-to-all-start.7) | async-done | bytes 1048608 | tf_op jit(solution)/shard_map/all_to_all | solution.py:23
  193.5 1.0 reduce_sum.139
  194.6 0.9 fusion.6
  (91 shorter events, 3.2 us)
Async XLA Ops:
  7.2 14.8 %copy-start = (bf16[16,256,128]{2,1,0:T(8,128)(2,1)S(1)}, bf16[16,256,128]{2,1,0:T(8,128)(2,1)}, u32[]{:S(2)}) copy-start(bf16[16,256,128]{2,1,0:T(8,128)(2,1)} %param.34) | copy-start | bytes 3145732
  7.2 12.6 %copy-start.5 = (bf16[128,1024]{1,0:T(8,128)(2,1)S(1)}, bf16[128,1024]{1,0:T(8,128)(2,1)}, u32[]{:S(2)}) copy-start(bf16[128,1024]{1,0:T(8,128)(2,1)} %param.32) | copy-start | bytes 786436
  7.2 13.1 %copy-start.10 = (f32[1024]{0:T(1024)S(1)}, f32[1024]{0:T(1024)}, u32[]{:S(2)}) copy-start(f32[1024]{0:T(1024)} %param.24) | copy-start | bytes 12292
  7.2 13.1 %copy-start.3 = (bf16[1024,128]{1,0:T(8,128)(2,1)S(1)}, bf16[1024,128]{1,0:T(8,128)(2,1)}, u32[]{:S(2)}) copy-start(bf16[1024,128]{1,0:T(8,128)(2,1)} %param.25) | copy-start | bytes 786436
  7.2 13.4 %copy-start.4 = (bf16[1024,128]{1,0:T(8,128)(2,1)S(1)}, bf16[1024,128]{1,0:T(8,128)(2,1)}, u32[]{:S(2)}) copy-start(bf16[1024,128]{1,0:T(8,128)(2,1)} %param.26) | copy-start | bytes 786436
  8.6 11.4 %all-to-all-start = ((bf16[4,16,256]{2,1,0:T(8,128)(2,1)}), bf16[4,16,256]{2,1,0:T(8,128)(2,1)S(1)}, u32[]{:S(2)}, u32[]{:S(2)}) async-start(bf16[4,16,256]{2,1,0:T(8,128)(2,1)} %broadcast_in_dim.25), calls=%async_computation | async-start | bytes 65536 | tf_op jit(solution)/shard_map/all_to_all | solution.py:23
  13.1 148.7 %all-gather.4.cloned.1.call-start = ((), (), s32[]{:S(2)}) async-start(), calls=%async_computation.8 | async-start | bytes 2113536 | tf_op jit(solution)/shard_map/all_gather | solution.py:57
  19.9 3.5 %copy-start.13 = (f32[128]{0:T(128)S(1)}, f32[128]{0:T(128)}, u32[]{:S(2)}) copy-start(f32[128]{0:T(128)} %param.31) | copy-start | bytes 1540
  20.2 9.1 %copy-start.11 = (f32[256]{0:T(256)S(1)}, f32[256]{0:T(256)}, u32[]{:S(2)}) copy-start(f32[256]{0:T(256)} %param.36) | copy-start | bytes 3076
  20.2 9.1 %copy-start.12 = (f32[256]{0:T(256)S(1)}, f32[256]{0:T(256)}, u32[]{:S(2)}) copy-start(f32[256]{0:T(256)} %param.45) | copy-start | bytes 3076
  20.3 14.4 %copy-start.6 = (bf16[16,256]{1,0:T(8,128)(2,1)S(1)}, bf16[16,256]{1,0:T(8,128)(2,1)}, u32[]{:S(2)}) copy-start(bf16[16,256]{1,0:T(8,128)(2,1)} %param.23) | copy-start | bytes 24580
  21.9 63.3 %copy-start.1 = (bf16[1,256,1024]{2,1,0:T(8,128)(2,1)S(1)}, bf16[1,256,1024]{2,1,0:T(8,128)(2,1)}, u32[]{:S(2)}) copy-start(bf16[1,256,1024]{2,1,0:T(8,128)(2,1)} %param.41) | copy-start | bytes 1572868
  23.4 62.0 %copy-start.9 = (bf16[16,128]{1,0:T(8,128)(2,1)}, bf16[16,128]{1,0:T(8,128)(2,1)S(1)}, u32[]{:S(2)}) copy-start(bf16[16,128]{1,0:T(8,128)(2,1)S(1)} %get-tuple-element.18) | copy-start | bytes 12292
  24.3 10.4 %all-to-all-start.1 = ((f32[4,16,256]{2,1,0:T(8,128)}), f32[4,16,256]{2,1,0:T(8,128)S(1)}, u32[]{:S(2)}, u32[]{:S(2)}) async-start(f32[4,16,256]{2,1,0:T(8,128)} %convolution_bitcast_fusion.3), calls=%async_computation.1 | async-start | bytes 131072 | tf_op jit(solution)/shard_map/all_to_all | solution.py:38
  35.5 8.4 %all-to-all-start.2 = ((f32[4,1,32]{2,1,0:T(1,128)}), f32[4,1,32]{2,1,0:T(1,128)S(1)}, u32[]{:S(2)}, u32[]{:S(2)}) async-start(f32[4,1,32]{2,1,0:T(1,128)} %broadcast_in_dim.27), calls=%async_computation.2 | async-start | bytes 4096 | tf_op jit(solution)/shard_map/all_to_all | solution.py:23
  81.6 14.4 %copy-start.2 = (bf16[1,1024,256]{2,1,0:T(8,128)(2,1)S(1)}, bf16[1,1024,256]{2,1,0:T(8,128)(2,1)}, u32[]{:S(2)}) copy-start(bf16[1,1024,256]{2,1,0:T(8,128)(2,1)} %param.39) | copy-start | bytes 1572868
  81.6 13.6 %all-to-all-start.4 = ((bf16[4,128,2,256]{3,2,1,0:T(2,128)(2,1)}), bf16[4,128,2,256]{3,2,1,0:T(2,128)(2,1)S(1)}, u32[]{:S(2)}, u32[]{:S(2)}) async-start(bf16[4,128,2,256]{3,2,1,0:T(2,128)(2,1)} %broadcast_in_dim.29), calls=%async_computation.4 | async-start | bytes 1048576 | tf_op jit(solution)/shard_map/all_to_all | solution.py:23
  85.4 10.9 %copy-start.15 = (bf16[1,1024,256]{2,1,0:T(8,128)(2,1)S(1)}, bf16[1,1024,256]{2,1,0:T(8,128)(2,1)}, u32[]{:S(2)}) copy-start(bf16[1,1024,256]{2,1,0:T(8,128)(2,1)} %param.40) | copy-start | bytes 1572868
  97.0 4.6 %copy-start.8 = (bf16[16,256]{1,0:T(8,128)(2,1)S(1)}, bf16[16,256]{1,0:T(8,128)(2,1)}, u32[]{:S(2)}) copy-start(bf16[16,256]{1,0:T(8,128)(2,1)} %param.44) | copy-start | bytes 24580
  98.1 47.2 %all-to-all-start.5 = ((f32[4,128,2,256]{3,1,2,0:T(8,128)}), f32[4,128,2,256]{3,1,2,0:T(8,128)S(1)}, u32[]{:S(2)}, u32[]{:S(2)}) async-start(f32[4,128,2,256]{3,1,2,0:T(8,128)} %copy.88), calls=%async_computation.5 | async-start | bytes 2097152 | tf_op jit(solution)/shard_map/all_to_all | solution.py:38
  101.6 78.7 %all-gather.6.cloned.1.call-start = ((), (), s32[]{:S(2)}) async-start(), calls=%async_computation.9 | async-start | bytes 1572864 | tf_op jit(solution)/shard_map/all_gather | solution.py:68
  146.2 25.7 %all-to-all-start.6 = ((bf16[128,2,256]{2,1,0:T(2,128)(2,1)}), bf16[128,2,256]{2,1,0:T(2,128)(2,1)S(1)}, u32[]{:S(2)}, u32[]{:S(2)}) async-start(bf16[128,2,256]{2,1,0:T(2,128)(2,1)} %copy.90), calls=%async_computation.6 | async-start | bytes 262144 | tf_op jit(solution)/shard_map/all_to_all | solution.py:241
  165.0 13.2 %copy-start.7 = (f32[16,6]{0,1:T(8,128)S(1)}, f32[16,6]{0,1:T(8,128)}, u32[]{:S(2)}) copy-start(f32[16,6]{0,1:T(8,128)} %param.38) | copy-start | bytes 1156
  165.1 13.4 %copy-start.14 = (f32[128]{0:T(128)S(1)}, f32[128]{0:T(128)}, u32[]{:S(2)}) copy-start(f32[128]{0:T(128)} %param.29) | copy-start | bytes 1540
  173.5 20.0 %all-to-all-start.7 = ((f32[4,1,65536]{2,1,0:T(1,128)}), f32[4,1,65536]{2,1,0:T(1,128)S(1)}, u32[]{:S(2)}, u32[]{:S(2)}) async-start(f32[4,1,65536]{2,1,0:T(1,128)} %broadcast_in_dim.30), calls=%async_computation.7 | async-start | bytes 2097152 | tf_op jit(solution)/shard_map/all_to_all | solution.py:23
Sparse Core Ops, SparseCore 0:
  17.0 144.7 all-gather.3
  163.9 16.4 all-gather.5
where the time goes:
time: 203 us; the launch traced here: 202 us
  blocking collectives  79.8 us (39%)
  waiting for transfers between devices  47 us (23%)
  starting transfers between devices  32.9 us (16%)
  between operations  15.2 us (7%)
  local copies, waits for them, and re-layouts  13.8 us (7%)
  matrix products  8.19 us (4%)
  other arithmetic  5.41 us (3%)
    all_gather x2, blocking collectives, stacked_from(): blocks = lax.all_gather(blocks, axes[k], axis=0, tiled=True)  43.6 us
    all_to_all x1, blocking collectives, body(): lax.all_to_all(placed.astype(jnp.bfloat16).reshape(experts, capacity, mix...  36.1 us
    all_to_all x4, waiting for transfers between devices, from_everyone(): return lax.all_to_all(copies, axis, split_axis=0, concat_axis=0, tiled=True)  26.5 us
    all_to_all x4, starting transfers between devices, from_everyone(): return lax.all_to_all(copies, axis, split_axis=0, concat_axis=0, tiled=True)  16 us
    all_to_all x1, starting transfers between devices, body(): lax.all_to_all(summed, EP, split_axis=0, concat_axis=0, tiled=True)  8.63 us
    all_to_all x2, starting transfers between devices, summed_on_arrival(): blocks = lax.all_to_all(cut_along(x, dim, length), axis, 0, 0, tiled=True)  8.31 us
    all_gather x1, waiting for transfers between devices, gather_turned(): whole, at, done = (lax.all_gather(both, axis, axis=0, tiled=True), 0, [])  6.94 us
    all_to_all x1, waiting for transfers between devices, body(): lax.all_to_all(summed, EP, split_axis=0, concat_axis=0, tiled=True)  6.83 us
  transfers between devices with their start and end apart: 9, of which 7 were waited for; matrix products, arithmetic and copies ran while one was open for 12% of the time, Pallas kernels for 0%

commit v1 on v0

--- a/solution.py
+++ b/solution.py
@@ -65,7 +65,9 @@
 def stacked_from(x, axes, sequence):
     blocks = x[None]
     for k in sequence:
-        blocks = lax.all_gather(blocks, axes[k], axis=0, tiled=True)
+        blocks = jnp.concatenate(
+            lax.all_to_all(jnp.stack([blocks] * lax.axis_size(axes[k])), axes[k], 0, 0), axis=0
+        )
     block = [lax.axis_size(axes[k]) for k in reversed(sequence)]
     blocks = blocks.reshape(*block, *x.shape)
     turned = sorted(range(len(sequence)), key=lambda place: sequence[len(sequence) - 1 - place])

time: 203 us -> 273 us (1.34)
  waiting for transfers between devices: 47 us -> 149 us
  blocking collectives: 79.8 us -> 16.1 us
  starting transfers between devices: 32.9 us -> 62.5 us
    all_gather x1, waiting for transfers between devices: 6.94 us -> 54.1 us  [gather_turned(): whole, at, done = (lax.all_gather(both, axis, axis=0, tiled=True), 0, [])]
    all_to_all x0 -> x4, waiting for transfers between devices: none -> 44.4 us  [the longest x3 28 us: stacked_from(): lax.all_to_all(jnp.stack([blocks] * lax.axis_size(axes[k])), axes[k], 0, 0)]
    all_gather x2 -> x0, blocking collectives: 43.6 us -> none  [stacked_from(): blocks = lax.all_gather(blocks, axes[k], axis=0, tiled=True)]
    all_to_all x0 -> x4, starting transfers between devices: none -> 29.7 us  [the longest x1 19 us: body(): lax.all_to_all(placed.astype(jnp.bfloat16).reshape(experts, capacity, mix...]
    all_to_all x1, blocking collectives: 36.1 us -> 16.1 us  [summed_on_arrival(): blocks = lax.all_to_all(cut_along(x, dim, length), axis, 0, 0, tiled=True)]
    all_to_all x1, waiting for transfers between devices: 6.83 us -> 17 us  [body(): lax.all_to_all(summed, EP, split_axis=0, concat_axis=0, tiled=True)]
    all_to_all x1, starting transfers between devices: 8.63 us -> 12.2 us  [body(): lax.all_to_all(summed, EP, split_axis=0, concat_axis=0, tiled=True)]
    all_to_all x2 -> x1, starting transfers between devices: 8.31 us -> 4.93 us  [summed_on_arrival(): blocks = lax.all_to_all(cut_along(x, dim, length), axis, 0, 0, tiled=True)]
  transfers between devices with their start and end apart: 9 -> 11, of which waited for: 7 -> 9; matrix products, arithmetic and copies ran while one was open for 12% -> 7% of each run, Pallas kernels for 0% -> 0%
where the time goes in v1:
time: 273 us; the launch traced here: 272 us
  waiting for transfers between devices  149 us (55%)
  starting transfers between devices  62.5 us (23%)
  blocking collectives  16.1 us (6%)
  between operations  15.3 us (6%)
  local copies, waits for them, and re-layouts  14.8 us (5%)
  matrix products  8.22 us (3%)
  other arithmetic  5.79 us (2%)
    all_gather x1, waiting for transfers between devices, gather_turned(): whole, at, done = (lax.all_gather(both, axis, axis=0, tiled=True), 0, [])  54.1 us
    all_to_all x3, waiting for transfers between devices, stacked_from(): lax.all_to_all(jnp.stack([blocks] * lax.axis_size(axes[k])), axes[k], 0, 0)  28 us
    all_to_all x4, waiting for transfers between devices, from_everyone(): return lax.all_to_all(copies, axis, split_axis=0, concat_axis=0, tiled=True)  28 us
    all_to_all x1, starting transfers between devices, body(): lax.all_to_all(placed.astype(jnp.bfloat16).reshape(experts, capacity, mix...  19 us
    all_to_all x1, waiting for transfers between devices, body(): lax.all_to_all(summed, EP, split_axis=0, concat_axis=0, tiled=True)  17 us
    all_to_all x1, waiting for transfers between devices, body(): lax.all_to_all(placed.astype(jnp.bfloat16).reshape(experts, capacity, mix...  16.4 us
    all_to_all x1, blocking collectives, summed_on_arrival(): blocks = lax.all_to_all(cut_along(x, dim, length), axis, 0, 0, tiled=True)  16.1 us
    all_to_all x4, starting transfers between devices, from_everyone(): return lax.all_to_all(copies, axis, split_axis=0, concat_axis=0, tiled=True)  15.6 us
  transfers between devices with their start and end apart: 11, of which 9 were waited for; matrix products, arithmetic and copies ran while one was open for 7% of the time, Pallas kernels for 0%

profile of v1, /device:TPU:32, one launch (start us, length us, event | category | flops | bytes accessed | tf_op | source)
XLA Modules:
  0.0 271.6 jit_solution(623000120929470631)
XLA Ops:
  7.2 1.4 broadcast_in_dim.23
  8.7 4.5 %all-to-all-start = ((bf16[4,16,256]{2,1,0:T(8,128)(2,1)}), bf16[4,16,256]{2,1,0:T(8,128)(2,1)S(1)}, u32[]{:S(2)}, u32[]{:S(2)}) async-start(bf16[4,16,256]{2,1,0:T(8,128)(2,1)} %broadcast_in_dim.23), calls=%async_computation | async-start | bytes 65536 | tf_op jit(solution)/shard_map/all_to_all | solution.py:23
  13.1 0.8 copy.76
  14.1 0.7 iota_compare_fusion.4
  14.8 0.7 mul.280
  15.5 0.7 mul.289
  16.3 1.5 copy.74
  20.1 0.2 fusion.25
  20.9 1.3 multiply_reduce_fusion.2
  22.2 0.8 convolution_bitcast_fusion.3
  23.0 4.9 %all-to-all-start.1 = ((f32[4,16,256]{2,1,0:T(8,128)}), f32[4,16,256]{2,1,0:T(8,128)S(1)}, u32[]{:S(2)}, u32[]{:S(2)}) async-start(f32[4,16,256]{2,1,0:T(8,128)} %convolution_bitcast_fusion.3), calls=%async_computation.1 | async-start | bytes 131072 | tf_op jit(solution)/shard_map/all_to_all | solution.py:38
  28.2 5.4 %all-to-all-done.1 = f32[4,16,256]{2,1,0:T(8,128)S(1)} async-done(((f32[4,16,256]{2,1,0:T(8,128)}), f32[4,16,256]{2,1,0:T(8,128)S(1)}, u32[]{:S(2)}, u32[]{:S(2)}) %all-to-all-start.1) | async-done | bytes 65568 | tf_op jit(solution)/shard_map/all_to_all | solution.py:38
  33.8 0.6 broadcast_in_dim.25
  34.4 3.2 %all-to-all-start.2 = ((f32[4,1,32]{2,1,0:T(1,128)}), f32[4,1,32]{2,1,0:T(1,128)S(1)}, u32[]{:S(2)}, u32[]{:S(2)}) async-start(f32[4,1,32]{2,1,0:T(1,128)} %broadcast_in_dim.25), calls=%async_computation.2 | async-start | bytes 4096 | tf_op jit(solution)/shard_map/all_to_all | solution.py:23
  37.6 5.2 %all-to-all-done.2 = f32[4,1,32]{2,1,0:T(1,128)S(1)} async-done(((f32[4,1,32]{2,1,0:T(1,128)}), f32[4,1,32]{2,1,0:T(1,128)S(1)}, u32[]{:S(2)}, u32[]{:S(2)}) %all-to-all-start.2) | async-done | bytes 544 | tf_op jit(solution)/shard_map/all_to_all | solution.py:23
  43.2 0.7 reshape.306
  43.9 19.0 %all-to-all-start.3 = ((bf16[128,2,256]{2,1,0:T(2,128)(2,1)}), bf16[128,2,256]{2,1,0:T(2,128)(2,1)S(1)}, u32[]{:S(2)}, u32[]{:S(2)}) async-start(bf16[128,2,256]{2,1,0:T(2,128)(2,1)} %reshape.306), calls=%async_computation.3 | async-start | bytes 262144 | tf_op jit(solution)/shard_map/all_to_all | solution.py:225
  63.0 0.6 pad_maximum_fusion.2
  63.7 16.4 %all-to-all-done.3 = bf16[128,2,256]{2,1,0:T(2,128)(2,1)S(1)} async-done(((bf16[128,2,256]{2,1,0:T(2,128)(2,1)}), bf16[128,2,256]{2,1,0:T(2,128)(2,1)S(1)}, u32[]{:S(2)}, u32[]{:S(2)}) %all-to-all-start.3) | async-done | bytes 131104 | tf_op jit(solution)/shard_map/all_to_all | solution.py:225
  80.0 1.1 broadcast_in_dim.27
  81.1 3.6 %all-to-all-start.4 = ((bf16[4,128,2,256]{3,2,1,0:T(2,128)(2,1)}), bf16[4,128,2,256]{3,2,1,0:T(2,128)(2,1)S(1)}, u32[]{:S(2)}, u32[]{:S(2)}) async-start(bf16[4,128,2,256]{3,2,1,0:T(2,128)(2,1)} %broadcast_in_dim.27), calls=%async_computation.4 | async-start | bytes 1048576 | tf_op jit(solution)/shard_map/all_to_all | solution.py:23
  84.9 9.8 %all-to-all-done.4 = bf16[4,128,2,256]{3,2,1,0:T(2,128)(2,1)S(1)} async-done(((bf16[4,128,2,256]{3,2,1,0:T(2,128)(2,1)}), bf16[4,128,2,256]{3,2,1,0:T(2,128)(2,1)S(1)}, u32[]{:S(2)}, u32[]{:S(2)}) %all-to-all-start.4) | async-done | bytes 524320 | tf_op jit(solution)/shard_map/all_to_all | solution.py:23
  94.7 0.6 stack.9
  95.3 3.3 %all-to-all-start.8 = ((bf16[4,1,16,256]{3,2,1,0:T(8,128)(2,1)}), bf16[4,1,16,256]{3,2,1,0:T(8,128)(2,1)S(1)}, u32[]{:S(2)}, u32[]{:S(2)}) async-start(bf16[4,1,16,256]{3,2,1,0:T(8,128)(2,1)} %stack.9), calls=%async_computation.8 | async-start | bytes 65536 | tf_op jit(solution)/shard_map/all_to_all | solution.py:69
  98.6 0.7 copy.78
  99.4 0.3 convolution_minimum_fusion
  99.7 0.3 fusion.3
  100.1 0.3 convolution_bitcast_fusion
  100.5 3.5 %all-to-all-done.8 = bf16[4,1,16,256]{3,2,1,0:T(8,128)(2,1)S(1)} async-done(((bf16[4,1,16,256]{3,2,1,0:T(8,128)(2,1)}), bf16[4,1,16,256]{3,2,1,0:T(8,128)(2,1)S(1)}, u32[]{:S(2)}, u32[]{:S(2)}) %all-to-all-start.8) | async-done | bytes 32800 | tf_op jit(solution)/shard_map/all_to_all | solution.py:69
  104.0 16.1 %all_to_all.57 = f32[4,128,2,256]{3,1,2,0:T(8,128)S(1)} all-to-all(f32[4,128,2,256]{3,1,2,0:T(8,128)S(1)} %copy.81), channel_id=1, replica_groups=mesh['ep_0'=16,'ep_1'=4,'ep_2'=2,'tp'=4] {'tp'}, dimensions={0} | all-to-all | bytes 2097152 | tf_op jit(solution)/shard_map/all_to_all | solution.py:38
  120.1 0.8 stack.10
  120.9 3.8 %all-to-all-start.9 = ((bf16[16,4,16,256]{3,2,1,0:T(8,128)(2,1)}), bf16[16,4,16,256]{3,2,1,0:T(8,128)(2,1)S(1)}, u32[]{:S(2)}, u32[]{:S(2)}) async-start(bf16[16,4,16,256]{3,2,1,0:T(8,128)(2,1)} %stack.10), calls=%async_computation.9 | async-start | bytes 1048576 | tf_op jit(solution)/shard_map/all_to_all | solution.py:69
  124.8 0.8 copy.83
  125.6 24.6 %all-to-all-done.9 = bf16[16,4,16,256]{3,2,1,0:T(8,128)(2,1)S(1)} async-done(((bf16[16,4,16,256]{3,2,1,0:T(8,128)(2,1)}), bf16[16,4,16,256]{3,2,1,0:T(8,128)(2,1)S(1)}, u32[]{:S(2)}, u32[]{:S(2)}) %all-to-all-start.9) | async-done | bytes 524320 | tf_op jit(solution)/shard_map/all_to_all | solution.py:69
  150.2 1.1 pad_maximum_fusion
  151.3 3.6 %all-to-all-start.10 = ((bf16[2,64,16,256]{3,2,1,0:T(8,128)(2,1)}), bf16[2,64,16,256]{3,2,1,0:T(8,128)(2,1)S(1)}, u32[]{:S(2)}, u32[]{:S(2)}) async-start(bf16[2,64,16,256]{3,2,1,0:T(8,128)(2,1)} %pad_maximum_fusion), calls=%async_computation.10 | async-start | bytes 2097152 | tf_op jit(solution)/shard_map/all_to_all | solution.py:69
  154.8 54.1 %all-gather.2.cloned.1.call-done = bf16[2048,512]{1,0:T(8,128)(2,1)} async-done(((bf16[16,512]{1,0:T(8,128)(2,1)}), bf16[2048,512]{1,0:T(8,128)(2,1)}) %all-gather.2.cloned.1.call-update) | async-done | bytes 2097168 | tf_op jit(solution)/shard_map/all_gather | solution.py:57
  208.9 1.6 convolution_bitcast_fusion.2
  210.5 1.6 convolution_bitcast_fusion.1
  212.2 12.2 %all-to-all-start.6 = ((bf16[128,2,256]{2,1,0:T(2,128)(2,1)}), bf16[128,2,256]{2,1,0:T(2,128)(2,1)S(1)}, u32[]{:S(2)}, u32[]{:S(2)}) async-start(bf16[128,2,256]{2,1,0:T(2,128)(2,1)} %copy.83), calls=%async_computation.6 | async-start | bytes 262144 | tf_op jit(solution)/shard_map/all_to_all | solution.py:243
  224.5 17.0 %all-to-all-done.6 = bf16[128,2,256]{2,1,0:T(2,128)(2,1)S(1)} async-done(((bf16[128,2,256]{2,1,0:T(2,128)(2,1)}), bf16[128,2,256]{2,1,0:T(2,128)(2,1)S(1)}, u32[]{:S(2)}, u32[]{:S(2)}) %all-to-all-start.6) | async-done | bytes 131104 | tf_op jit(solution)/shard_map/all_to_all | solution.py:243
  241.6 1.6 broadcast_in_dim.28
  243.1 4.3 %all-to-all-start.7 = ((f32[4,1,65536]{2,1,0:T(1,128)}), f32[4,1,65536]{2,1,0:T(1,128)S(1)}, u32[]{:S(2)}, u32[]{:S(2)}) async-start(f32[4,1,65536]{2,1,0:T(1,128)} %broadcast_in_dim.28), calls=%async_computation.7 | async-start | bytes 2097152 | tf_op jit(solution)/shard_map/all_to_all | solution.py:23
  247.8 0.6 multiply_convert_fusion.6
  248.4 1.1 copy.86
  249.7 13.0 %all-to-all-done.7 = f32[4,1,65536]{2,1,0:T(1,128)S(1)} async-done(((f32[4,1,65536]{2,1,0:T(1,128)}), f32[4,1,65536]{2,1,0:T(1,128)S(1)}, u32[]{:S(2)}, u32[]{:S(2)}) %all-to-all-start.7) | async-done | bytes 1048608 | tf_op jit(solution)/shard_map/all_to_all | solution.py:23
  262.8 1.0 reduce_sum.139
  263.9 0.9 fusion.6
  (101 shorter events, 4.4 us)
Async XLA Ops:
  7.2 13.4 %copy-start = (bf16[16,256,128]{2,1,0:T(8,128)(2,1)S(1)}, bf16[16,256,128]{2,1,0:T(8,128)(2,1)}, u32[]{:S(2)}) copy-start(bf16[16,256,128]{2,1,0:T(8,128)(2,1)} %param.34) | copy-start | bytes 3145732
  7.2 11.2 %copy-start.6 = (bf16[128,1024]{1,0:T(8,128)(2,1)S(1)}, bf16[128,1024]{1,0:T(8,128)(2,1)}, u32[]{:S(2)}) copy-start(bf16[128,1024]{1,0:T(8,128)(2,1)} %param.32) | copy-start | bytes 786436
  7.2 11.7 %copy-start.13 = (f32[1024]{0:T(1024)S(1)}, f32[1024]{0:T(1024)}, u32[]{:S(2)}) copy-start(f32[1024]{0:T(1024)} %param.24) | copy-start | bytes 12292
  7.2 11.8 %copy-start.4 = (bf16[1024,128]{1,0:T(8,128)(2,1)S(1)}, bf16[1024,128]{1,0:T(8,128)(2,1)}, u32[]{:S(2)}) copy-start(bf16[1024,128]{1,0:T(8,128)(2,1)} %param.25) | copy-start | bytes 786436
  7.2 12.1 %copy-start.5 = (bf16[1024,128]{1,0:T(8,128)(2,1)S(1)}, bf16[1024,128]{1,0:T(8,128)(2,1)}, u32[]{:S(2)}) copy-start(bf16[1024,128]{1,0:T(8,128)(2,1)} %param.26) | copy-start | bytes 786436
  8.7 10.1 %all-to-all-start = ((bf16[4,16,256]{2,1,0:T(8,128)(2,1)}), bf16[4,16,256]{2,1,0:T(8,128)(2,1)S(1)}, u32[]{:S(2)}, u32[]{:S(2)}) async-start(bf16[4,16,256]{2,1,0:T(8,128)(2,1)} %broadcast_in_dim.23), calls=%async_computation | async-start | bytes 65536 | tf_op jit(solution)/shard_map/all_to_all | solution.py:23
  18.6 3.6 %copy-start.16 = (f32[128]{0:T(128)S(1)}, f32[128]{0:T(128)}, u32[]{:S(2)}) copy-start(f32[128]{0:T(128)} %param.31) | copy-start | bytes 1540
  18.9 9.2 %copy-start.14 = (f32[256]{0:T(256)S(1)}, f32[256]{0:T(256)}, u32[]{:S(2)}) copy-start(f32[256]{0:T(256)} %param.36) | copy-start | bytes 3076
  18.9 9.3 %copy-start.15 = (f32[256]{0:T(256)S(1)}, f32[256]{0:T(256)}, u32[]{:S(2)}) copy-start(f32[256]{0:T(256)} %param.45) | copy-start | bytes 3076
  19.0 14.6 %copy-start.7 = (bf16[16,256]{1,0:T(8,128)(2,1)S(1)}, bf16[16,256]{1,0:T(8,128)(2,1)}, u32[]{:S(2)}) copy-start(bf16[16,256]{1,0:T(8,128)(2,1)} %param.23) | copy-start | bytes 24580
  20.1 42.8 %copy-start.10 = (bf16[256,16]{0,1:T(8,128)(2,1)S(1)}, bf16[256,16]{0,1:T(8,128)(2,1)}, u32[]{:S(2)}) copy-start(bf16[256,16]{0,1:T(8,128)(2,1)} %param.43) | copy-start | bytes 24580
  20.1 42.9 %copy-start.11 = (bf16[256,16]{0,1:T(8,128)(2,1)S(1)}, bf16[256,16]{0,1:T(8,128)(2,1)}, u32[]{:S(2)}) copy-start(bf16[256,16]{0,1:T(8,128)(2,1)} %param.42) | copy-start | bytes 24580
  20.9 63.9 %copy-start.2 = (bf16[1,256,1024]{2,1,0:T(8,128)(2,1)S(1)}, bf16[1,256,1024]{2,1,0:T(8,128)(2,1)}, u32[]{:S(2)}) copy-start(bf16[1,256,1024]{2,1,0:T(8,128)(2,1)} %param.41) | copy-start | bytes 1572868
  22.2 62.8 %copy-start.12 = (bf16[16,128]{1,0:T(8,128)(2,1)}, bf16[16,128]{1,0:T(8,128)(2,1)S(1)}, u32[]{:S(2)}) copy-start(bf16[16,128]{1,0:T(8,128)(2,1)S(1)} %get-tuple-element.18) | copy-start | bytes 12292
  23.0 71.7 %copy-start.9 = (bf16[16,256]{1,0:T(8,128)(2,1)S(1)}, bf16[16,256]{1,0:T(8,128)(2,1)}, u32[]{:S(2)}) copy-start(bf16[16,256]{1,0:T(8,128)(2,1)} %param.44) | copy-start | bytes 24580
  23.0 10.6 %all-to-all-start.1 = ((f32[4,16,256]{2,1,0:T(8,128)}), f32[4,16,256]{2,1,0:T(8,128)S(1)}, u32[]{:S(2)}, u32[]{:S(2)}) async-start(f32[4,16,256]{2,1,0:T(8,128)} %convolution_bitcast_fusion.3), calls=%async_computation.1 | async-start | bytes 131072 | tf_op jit(solution)/shard_map/all_to_all | solution.py:38
  34.4 8.4 %all-to-all-start.2 = ((f32[4,1,32]{2,1,0:T(1,128)}), f32[4,1,32]{2,1,0:T(1,128)S(1)}, u32[]{:S(2)}, u32[]{:S(2)}) async-start(f32[4,1,32]{2,1,0:T(1,128)} %broadcast_in_dim.25), calls=%async_computation.2 | async-start | bytes 4096 | tf_op jit(solution)/shard_map/all_to_all | solution.py:23
  43.9 36.1 %all-to-all-start.3 = ((bf16[128,2,256]{2,1,0:T(2,128)(2,1)}), bf16[128,2,256]{2,1,0:T(2,128)(2,1)S(1)}, u32[]{:S(2)}, u32[]{:S(2)}) async-start(bf16[128,2,256]{2,1,0:T(2,128)(2,1)} %reshape.306), calls=%async_computation.3 | async-start | bytes 262144 | tf_op jit(solution)/shard_map/all_to_all | solution.py:225
  62.9 146.0 %all-gather.2.cloned.1.call-start = ((), (), s32[]{:S(2)}) async-start(), calls=%async_computation.11 | async-start | bytes 2113536 | tf_op jit(solution)/shard_map/all_gather | solution.py:57
  81.1 18.3 %copy-start.3 = (bf16[1,1024,256]{2,1,0:T(8,128)(2,1)S(1)}, bf16[1,1024,256]{2,1,0:T(8,128)(2,1)}, u32[]{:S(2)}) copy-start(bf16[1,1024,256]{2,1,0:T(8,128)(2,1)} %param.39) | copy-start | bytes 1572868
  81.1 13.6 %all-to-all-start.4 = ((bf16[4,128,2,256]{3,2,1,0:T(2,128)(2,1)}), bf16[4,128,2,256]{3,2,1,0:T(2,128)(2,1)S(1)}, u32[]{:S(2)}, u32[]{:S(2)}) async-start(bf16[4,128,2,256]{3,2,1,0:T(2,128)(2,1)} %broadcast_in_dim.27), calls=%async_computation.4 | async-start | bytes 1048576 | tf_op jit(solution)/shard_map/all_to_all | solution.py:23
  84.9 14.8 %copy-start.18 = (bf16[1,1024,256]{2,1,0:T(8,128)(2,1)S(1)}, bf16[1,1024,256]{2,1,0:T(8,128)(2,1)}, u32[]{:S(2)}) copy-start(bf16[1,1024,256]{2,1,0:T(8,128)(2,1)} %param.40) | copy-start | bytes 1572868
  95.3 8.7 %all-to-all-start.8 = ((bf16[4,1,16,256]{3,2,1,0:T(8,128)(2,1)}), bf16[4,1,16,256]{3,2,1,0:T(8,128)(2,1)S(1)}, u32[]{:S(2)}, u32[]{:S(2)}) async-start(bf16[4,1,16,256]{3,2,1,0:T(8,128)(2,1)} %stack.9), calls=%async_computation.8 | async-start | bytes 65536 | tf_op jit(solution)/shard_map/all_to_all | solution.py:69
  120.9 29.3 %all-to-all-start.9 = ((bf16[16,4,16,256]{3,2,1,0:T(8,128)(2,1)}), bf16[16,4,16,256]{3,2,1,0:T(8,128)(2,1)S(1)}, u32[]{:S(2)}, u32[]{:S(2)}) async-start(bf16[16,4,16,256]{3,2,1,0:T(8,128)(2,1)} %stack.10), calls=%async_computation.9 | async-start | bytes 1048576 | tf_op jit(solution)/shard_map/all_to_all | solution.py:69
  151.3 60.9 %all-to-all-start.10 = ((bf16[2,64,16,256]{3,2,1,0:T(8,128)(2,1)}), bf16[2,64,16,256]{3,2,1,0:T(8,128)(2,1)S(1)}, u32[]{:S(2)}, u32[]{:S(2)}) async-start(bf16[2,64,16,256]{3,2,1,0:T(8,128)(2,1)} %pad_maximum_fusion), calls=%async_computation.10 | async-start | bytes 2097152 | tf_op jit(solution)/shard_map/all_to_all | solution.py:69
  212.2 35.3 %copy-start.8 = (f32[16,6]{0,1:T(8,128)S(1)}, f32[16,6]{0,1:T(8,128)}, u32[]{:S(2)}) copy-start(f32[16,6]{0,1:T(8,128)} %param.38) | copy-start | bytes 1156
  212.2 29.3 %all-to-all-start.6 = ((bf16[128,2,256]{2,1,0:T(2,128)(2,1)}), bf16[128,2,256]{2,1,0:T(2,128)(2,1)S(1)}, u32[]{:S(2)}, u32[]{:S(2)}) async-start(bf16[128,2,256]{2,1,0:T(2,128)(2,1)} %copy.83), calls=%async_computation.6 | async-start | bytes 262144 | tf_op jit(solution)/shard_map/all_to_all | solution.py:243
  224.5 23.3 %copy-start.17 = (f32[128]{0:T(128)S(1)}, f32[128]{0:T(128)}, u32[]{:S(2)}) copy-start(f32[128]{0:T(128)} %param.29) | copy-start | bytes 1540
  243.1 19.7 %all-to-all-start.7 = ((f32[4,1,65536]{2,1,0:T(1,128)}), f32[4,1,65536]{2,1,0:T(1,128)S(1)}, u32[]{:S(2)}, u32[]{:S(2)}) async-start(f32[4,1,65536]{2,1,0:T(1,128)} %broadcast_in_dim.28), calls=%async_computation.7 | async-start | bytes 2097152 | tf_op jit(solution)/shard_map/all_to_all | solution.py:23
  249.5 14.3 %copy-start.1 = (bf16[2,64,16,256]{3,2,0,1:T(8,128)(2,1)S(1)}, bf16[2,64,16,256]{3,2,0,1:T(8,128)(2,1)}, u32[]{:S(2)}) copy-start(bf16[2,64,16,256]{3,2,0,1:T(8,128)(2,1)} %copy.86) | copy-start | bytes 3145732
Sparse Core Ops, SparseCore 0:
  66.9 141.9 all-gather.1
